TPU v7x, 32 devices: a whole 2x2x4 slice. The times are simulated.
32 devices in a mesh: sp: 4 (over z), fs: 4 (over y, x), tp: 2 (over core).
Axes of the slice: x: 2, y: 2, z: 4, core: 2. Of those that a mesh axis runs over, the one named last changes fastest.
Arguments:
- tokens: bfloat16 [4, 640, 2048], P('fs', 'sp', 'tp'), may hold values from -6 to 6
- mix_gain: float32 [2048], replicated, may hold values from 0.1 to 1.9
- conv_b_weight: bfloat16 [2048, 1024], P(('sp', 'fs'), 'tp'), may hold values from -0.125 to 0.125
- conv_c_weight: bfloat16 [2048, 1024], P(('sp', 'fs'), 'tp'), may hold values from -0.125 to 0.125
- conv_v_weight: bfloat16 [2048, 1024], P(('sp', 'fs'), 'tp'), may hold values from -0.125 to 0.125
- conv_taps: float32 [3, 1024], P(None, 'tp'), may hold values from -3.5 to 3.5
- query_weight: bfloat16 [2048, 2048], P(('sp', 'fs'), 'tp'), may hold values from -0.125 to 0.125
- query_rope_weight: bfloat16 [2048, 1024], P(('sp', 'fs'), 'tp'), may hold values from -4.5 to 4.5
- latent_weight: bfloat16 [2048, 512], P(('sp', 'fs')), may hold values from -0.125 to 0.125
- key_rope_weight: bfloat16 [2048, 64], replicated, may hold values from -1 to 1
- latent_gain: float32 [512], replicated, may hold values from 0.1 to 1.9
- key_up_weight: bfloat16 [512, 2048], P(None, 'tp'), may hold values from -0.25 to 0.25
- value_up_weight: bfloat16 [512, 2048], P(None, 'tp'), may hold values from -0.25 to 0.25
- head_gain: float32 [2048], P('tp'), may hold values from 0.1 to 1.9
- conv_out_weight: bfloat16 [1024, 2048], P('tp', ('sp', 'fs')), may hold values from -0.109375 to 0.109375
- attn_out_weight: bfloat16 [2048, 2048], P('tp', ('sp', 'fs')), may hold values from -0.109375 to 0.109375
Outputs:
- mixed: bfloat16 [4, 640, 2048], P('fs', ('sp', 'tp'))
All inputs are finite; a program needn't handle non-finite values.
Results may differ from a plain program's by a relative error of at most 0.025.
Values may be sent and summed in bfloat16 or wider, within the bound.
No kernel may reach another device: no remote copies, remote signals or barrier semaphores. Data moves between devices by JAX's collectives and lax.ppermute only.
A program may use at most 128 MiB of HBM per device.

v0:
```python
import jax
import jax.numpy as jnp
from jax import lax
from jax.sharding import PartitionSpec as P

NOPE = 128
ROPE = 64
VD = 128
KVL = 512
SEG = 64
norm_epsilon = 1e-06
rope_theta = 10000.0


def passed_along(block, axis, distance):
    devices = range(lax.axis_size(axis))
    route = [(i - distance, i) for i in devices if i - distance in devices]
    return lax.ppermute(block, axis, route)


def rms_scale(values, gain):
    return (
        values * lax.rsqrt(jnp.mean(values * values, axis=-1, keepdims=True) + norm_epsilon) * gain
    )


def rope_tables(positions):
    half_width = ROPE // 2
    frequency = rope_theta ** (-jnp.arange(half_width, dtype=jnp.float32) * 2.0 / ROPE)
    angles = positions[:, None] * frequency[None, :]
    return (jnp.cos(angles), jnp.sin(angles))


def rotate(values, cosine, sine):
    half_width = ROPE // 2
    first = values[..., :half_width]
    second = values[..., half_width:]
    return jnp.concatenate(
        [first * cosine - second * sine, second * cosine + first * sine], axis=-1
    )


def shards(
    tokens,
    mix_gain,
    conv_b_weight,
    conv_c_weight,
    conv_v_weight,
    conv_taps,
    query_weight,
    query_rope_weight,
    latent_weight,
    key_rope_weight,
    latent_gain,
    key_up_weight,
    value_up_weight,
    head_gain,
    conv_out_weight,
    attn_out_weight,
):
    full_rows = lax.all_gather(tokens[0], "tp", axis=1, tiled=True)
    tok_rows = full_rows.shape[0]
    normed = rms_scale(full_rows.astype(jnp.float32), mix_gain).astype(jnp.bfloat16)
    offset = lax.axis_index("sp") * tok_rows
    token_index = offset + jnp.arange(tok_rows, dtype=jnp.int32)
    cosine, sine = rope_tables(token_index.astype(jnp.float32))
    local_heads = query_weight.shape[1] // NOPE
    count_sp = lax.axis_size("sp")
    count_fs = lax.axis_size("fs")
    count_tp = lax.axis_size("tp")
    fs_index = lax.axis_index("fs")
    row_piece = normed.shape[1] // (count_sp * count_fs)
    all_normed = lax.all_gather(normed, "fs", axis=0, tiled=True)
    picked = lax.dynamic_index_in_dim(
        all_normed.reshape(-1, count_sp, count_fs, row_piece), fs_index, 2, keepdims=False
    ).reshape(-1, count_sp * row_piece)
    gathered = (
        lax.all_gather(conv_b_weight, "sp", axis=0, tiled=True),
        lax.all_gather(conv_c_weight, "sp", axis=0, tiled=True),
        lax.all_gather(conv_v_weight, "sp", axis=0, tiled=True),
        lax.all_gather(query_weight, "sp", axis=0, tiled=True),
        lax.all_gather(query_rope_weight, "sp", axis=0, tiled=True),
        lax.all_gather(latent_weight, "sp", axis=0, tiled=True),
    )

    def project_in():
        return jnp.concatenate(
            [jnp.dot(picked, member, preferred_element_type=jnp.float32) for member in gathered],
            axis=1,
        )

    joined = lax.psum_scatter(
        project_in().astype(jnp.bfloat16), "fs", scatter_dimension=0, tiled=True
    ).astype(jnp.float32)
    bounds = []
    running_total = 0
    for member in gathered[:-1]:
        running_total = running_total + member.shape[1]
        bounds.append(running_total)
    sums = tuple(jnp.split(joined, bounds, axis=1))
    latent_raw = sums[5].astype(jnp.bfloat16)
    gate_b = sums[0].astype(jnp.bfloat16)
    gate_c = sums[1].astype(jnp.bfloat16)
    values_v = sums[2].astype(jnp.bfloat16)
    query_nope = sums[3].astype(jnp.bfloat16).reshape(tok_rows, local_heads, NOPE)
    query_rot = rotate(
        sums[4].reshape(tok_rows, local_heads, ROPE), cosine[:, None, :], sine[:, None, :]
    ).astype(jnp.bfloat16)
    latent = rms_scale(latent_raw.astype(jnp.float32), latent_gain).astype(jnp.bfloat16)
    key_rot = rotate(
        jnp.dot(normed, key_rope_weight, preferred_element_type=jnp.float32), cosine, sine
    ).astype(jnp.bfloat16)
    query_latent = jnp.einsum(
        "thn,khn->thk",
        query_nope,
        key_up_weight.reshape(KVL, local_heads, NOPE),
        preferred_element_type=jnp.float32,
    ).astype(jnp.bfloat16)
    attn_scale = (NOPE + ROPE) ** (-0.5)
    product = (gate_c.astype(jnp.float32) * values_v.astype(jnp.float32)).astype(jnp.bfloat16)
    previous = passed_along(product[tok_rows - 2 :], "sp", 1)
    padded = jnp.concatenate([previous, product], axis=0).astype(jnp.float32)
    convolved = (
        conv_taps[0] * padded[0:tok_rows]
        + conv_taps[1] * padded[1 : tok_rows + 1]
        + conv_taps[2] * padded[2 : tok_rows + 2]
    )
    conv_y = (gate_b.astype(jnp.float32) * convolved).astype(jnp.bfloat16)
    query_segment = token_index // SEG
    last_segment = (offset + tok_rows - 1) // SEG

    def key_block(running, latent_block, rot_block, first_key):
        peak_old, denom_old, accum_old = running
        block_rows = latent_block.shape[0]
        scores = (
            jnp.einsum(
                "thk,jk->thj", query_latent, latent_block, preferred_element_type=jnp.float32
            )
            + jnp.einsum("thr,jr->thj", query_rot, rot_block, preferred_element_type=jnp.float32)
        ) * attn_scale
        key_segment = (first_key + jnp.arange(block_rows, dtype=jnp.int32)) // SEG
        allowed = key_segment[None, None, :] <= query_segment[:, None, None]
        peak_new = jnp.maximum(peak_old, jnp.max(jnp.where(allowed, scores, -1e30), axis=-1))
        weights = jnp.where(allowed, jnp.exp(scores - peak_new[..., None]), 0.0)
        rescale = jnp.exp(peak_old - peak_new)
        denom_new = denom_old * rescale + jnp.sum(weights, axis=-1)
        accum_new = accum_old * rescale[..., None] + jnp.einsum(
            "thj,jk->thk",
            weights.astype(jnp.bfloat16),
            latent_block,
            preferred_element_type=jnp.float32,
        )
        return (peak_new, denom_new, accum_new)

    starting = (
        jnp.full((tok_rows, local_heads), -1e30, jnp.float32),
        jnp.zeros((tok_rows, local_heads), jnp.float32),
        jnp.zeros((tok_rows, local_heads, KVL), jnp.float32),
    )
    latent_piece = lax.all_gather(latent, "sp", axis=0, tiled=True)
    rot_piece = lax.all_gather(key_rot, "sp", axis=0, tiled=True)
    piece_rows = latent_piece.shape[0]
    splits = max(1, piece_rows // 512)
    while piece_rows % splits:
        splits = splits - 1
    block_rows = piece_rows // splits

    def visit(state, block_index):
        block_begin = block_index * block_rows
        latent_block = lax.dynamic_slice_in_dim(latent_piece, block_begin, block_rows, 0)
        rot_block = lax.dynamic_slice_in_dim(rot_piece, block_begin, block_rows, 0)
        updated = lax.cond(
            block_begin // SEG <= last_segment,
            lambda inner: key_block(inner, latent_block, rot_block, block_begin),
            lambda inner: inner,
            state,
        )
        return (updated, None)

    peak, denom, accum = lax.scan(visit, starting, jnp.arange(splits, dtype=jnp.int32))[0]
    attended = (accum / denom[..., None]).astype(jnp.bfloat16)
    head_out = jnp.einsum(
        "thk,khv->thv",
        attended,
        value_up_weight.reshape(KVL, local_heads, VD),
        preferred_element_type=jnp.float32,
    )
    normed_heads = rms_scale(head_out, head_gain.reshape(local_heads, VD))
    attn_y = normed_heads.astype(jnp.bfloat16).reshape(tok_rows, local_heads * VD)
    share_rows = tok_rows // count_tp
    conv_all, attn_all = (
        lax.all_gather(conv_y, "fs", axis=0, tiled=True),
        lax.all_gather(attn_y, "fs", axis=0, tiled=True),
    )
    conv_sorted = (
        conv_all.reshape(count_fs, count_tp, share_rows, -1)
        .transpose(1, 0, 2, 3)
        .reshape(count_fs * tok_rows, -1)
    )
    attn_sorted = (
        attn_all.reshape(count_fs, count_tp, share_rows, -1)
        .transpose(1, 0, 2, 3)
        .reshape(count_fs * tok_rows, -1)
    )
    conv_cols_sp, attn_cols_sp = (
        lax.all_gather(conv_out_weight, "sp", axis=1, tiled=True),
        lax.all_gather(attn_out_weight, "sp", axis=1, tiled=True),
    )
    col_sums = lax.psum_scatter(
        (
            jnp.dot(conv_sorted, conv_cols_sp, preferred_element_type=jnp.float32)
            + jnp.dot(attn_sorted, attn_cols_sp, preferred_element_type=jnp.float32)
        ).astype(jnp.bfloat16),
        "tp",
        scatter_dimension=0,
        tiled=True,
    )
    col_piece = conv_cols_sp.shape[1] // count_sp
    outgoing = col_sums.reshape(count_fs, share_rows, count_sp * col_piece)
    arrived = lax.all_to_all(outgoing, "fs", split_axis=0, concat_axis=2, tiled=True)
    result = (
        arrived.reshape(share_rows, count_fs, count_sp, col_piece)
        .transpose(0, 2, 1, 3)
        .reshape(share_rows, count_fs * count_sp * col_piece)
    )
    return result[None]


def solution(mesh):
    return jax.shard_map(
        shards,
        mesh=mesh,
        in_specs=(
            P("fs", "sp", "tp"),
            P(),
            P(("sp", "fs"), "tp"),
            P(("sp", "fs"), "tp"),
            P(("sp", "fs"), "tp"),
            P(None, "tp"),
            P(("sp", "fs"), "tp"),
            P(("sp", "fs"), "tp"),
            P(("sp", "fs"), None),
            P(),
            P(),
            P(None, "tp"),
            P(None, "tp"),
            P("tp"),
            P("tp", ("sp", "fs")),
            P("tp", ("sp", "fs")),
        ),
        out_specs=P("fs", ("sp", "tp"), None),
        check_vma=False,
    )
```

profile of v0, /device:TPU:0, one launch (start us, length us, event | category | flops | bytes accessed | tf_op | source)
XLA Modules:
  0.0 311.9 jit_solution(16413146177102707444)
XLA Ops:
  6.6 2.7 all-gather
  12.2 17.5 %all_gather.44 = bf16[512,512]{1,0:T(8,128)(2,1)S(1)} all-gather(bf16[128,512]{1,0:T(8,128)(2,1)S(1)} %copy-done.9), channel_id=1, replica_groups=mesh['sp'=4,'fs'=4,'tp'=2] {'sp'}, dimensions={0}, use_global_device_ids=true | all-gather | bytes 655360 | tf_op jit(solution)/shard_map/all_gather | solution.py:78
  29.6 16.5 %all_gather.45 = bf16[512,512]{1,0:T(8,128)(2,1)} all-gather(bf16[128,512]{1,0:T(8,128)(2,1)S(1)} %copy-done.10), channel_id=1, replica_groups=mesh['sp'=4,'fs'=4,'tp'=2] {'sp'}, dimensions={0}, use_global_device_ids=true | all-gather | bytes 655360 | tf_op jit(solution)/shard_map/all_gather | solution.py:79
  46.1 16.7 %all_gather.46 = bf16[512,512]{1,0:T(8,128)(2,1)} all-gather(bf16[128,512]{1,0:T(8,128)(2,1)S(1)} %copy-done.11), channel_id=1, replica_groups=mesh['sp'=4,'fs'=4,'tp'=2] {'sp'}, dimensions={0}, use_global_device_ids=true | all-gather | bytes 655360 | tf_op jit(solution)/shard_map/all_gather | solution.py:80
  62.8 22.8 %all_gather.48 = bf16[512,512]{1,0:T(8,128)(2,1)S(1)} all-gather(bf16[128,512]{1,0:T(8,128)(2,1)S(1)} %copy-done.12), channel_id=1, replica_groups=mesh['sp'=4,'fs'=4,'tp'=2] {'sp'}, dimensions={0}, use_global_device_ids=true | all-gather | bytes 655360 | tf_op jit(solution)/shard_map/all_gather | solution.py:82
  85.6 17.8 %all_gather.49 = bf16[512,512]{1,0:T(8,128)(2,1)} all-gather(bf16[128,512]{1,0:T(8,128)(2,1)S(1)} %copy-done.13), channel_id=1, replica_groups=mesh['sp'=4,'fs'=4,'tp'=2] {'sp'}, dimensions={0}, use_global_device_ids=true | all-gather | bytes 655360 | tf_op jit(solution)/shard_map/all_gather | solution.py:83
  103.4 4.4 %copy.65 = bf16[640,2048]{0,1:T(8,128)(2,1)} copy(bf16[640,2048]{1,0:T(8,128)(2,1)} %all-gather.7.cloned.1.call-done) | data formatting | bytes 5242880 | tf_op jit(solution)/shard_map/all_gather | solution.py:73
  109.9 2.5 convolution_convert_fusion.5
  113.8 2.5 convolution_convert_fusion.4
  120.4 3.3 %fusion.15 = bf16[640,3584]{1,0:T(8,128)(2,1)} fusion(bf16[640,3584]{1,0:T(8,128)(2,1)} %constant_dynamic-update-slice_fusion, bf16[640,512]{0,1:T(8,128)(2,1)S(1)} %bitcast.104, bf16[512,1024]{1,0:T(8,128)(2,1)} %all-gather.9.cloned.1.call-done), kind=kOutput, calls=%fused_computation.35 | convolution fusion | flops 671744000 | bytes 3014656 | tf_op jit(solution)/shard_map/dot_general | solution.py:88
  130.3 14.1 %all-gather.1 = bf16[4,160,64]{1,2,0:T(8,128)(2,1)} all-gather(bf16[1,160,64]{1,2,0:T(8,128)(2,1)S(1)} %maximum_bitcast_fusion), channel_id=1, replica_groups=mesh['sp'=4,'fs'=4,'tp'=2] {'sp'}, dimensions={0}, use_global_device_ids=true | all-gather | bytes 102400 | tf_op jit(solution)/shard_map/all_gather | solution.py:161
  144.3 36.4 %reduce-scatter.3.cloned.1.call-done = bf16[160,3584]{1,0:T(8,128)(2,1)} async-done(((bf16[640,3584]{1,0:T(8,128)(2,1)}), bf16[160,3584]{1,0:T(8,128)(2,1)}) %reduce-scatter.3.cloned.1.call-update) | async-done | bytes 1146896 | tf_op jit(solution)/shard_map/reduce_scatter | solution.py:92
  183.6 17.8 %all_gather.52 = bf16[640,512]{1,0:T(8,128)(2,1)S(1)} all-gather(bf16[160,512]{1,0:T(8,128)(2,1)S(1)} %get-tuple-element.251), channel_id=1, replica_groups=mesh['sp'=4,'fs'=4,'tp'=2] {'sp'}, dimensions={0}, use_global_device_ids=true | all-gather | bytes 819200 | tf_op jit(solution)/shard_map/all_gather | solution.py:160
  204.5 12.2 %conditional.1 = ((f32[160,8]{1,0:T(8,128)S(1)}, f32[160,8,512]{2,1,0:T(8,128)})) conditional(s32[]{:T(128)} %convert_element_type.79, (f32[160,8]{1,0:T(8,128)S(1)}, f32[160,8,512]{2,1,0:T(8,128)}) %tuple.31, (s32[160]{0:T(256)S(1)}, s32[160]{0:T(256)S(1)}, s32[]{:T(128)}, bf16[160,8,512]{2,0,1:T(8,128)(2,1)S(1)}, ...), branch_computations={%region_3.4_spmd, %region_4.7_spmd.clone} | conditional | flops 1792195712 | bytes 46272084 | solution.py:172
  209.7 1.9 select_reduce_fusion
  216.7 2.1 divide_convert_fusion
  221.6 2.5 collective-permute-start
  224.1 15.4 %all_gather.51 = bf16[512,512]{1,0:T(8,128)(2,1)S(1)} all-gather(bf16[512,128]{1,0:T(8,128)(2,1)S(1)} %copy-done.14), channel_id=1, replica_groups=mesh['sp'=4,'fs'=4,'tp'=2] {'sp'}, dimensions={1}, use_global_device_ids=true | all-gather | bytes 655360 | tf_op jit(solution)/shard_map/all_gather | solution.py:206
  240.6 12.5 %all_gather.50 = bf16[640,512]{1,0:T(8,128)(2,1)S(1)} all-gather(bf16[160,512]{1,0:T(8,128)(2,1)S(1)} %fusion.40), channel_id=1, replica_groups=mesh['sp'=4,'fs'=4,'tp'=2] {'fs'}, dimensions={0}, use_global_device_ids=true | all-gather | bytes 819200 | tf_op jit(solution)/shard_map/all_gather | solution.py:192
  253.6 2.5 copy.81
  256.1 26.6 %all-gather.13.cloned.1.call-done = bf16[1024,512]{1,0:T(8,128)(2,1)} async-done(((bf16[1024,128]{1,0:T(8,128)(2,1)}), bf16[1024,512]{1,0:T(8,128)(2,1)}) %all-gather.13.cloned.1.call-update) | async-done | bytes 1048592 | tf_op jit(solution)/shard_map/all_gather | solution.py:207
  282.8 3.3 %fusion.17 = bf16[640,512]{1,0:T(8,128)(2,1)} fusion(f32[640,512]{1,0:T(8,128)S(1)} %fusion.44, bf16[640,1024]{1,0:T(8,128)(2,1)} %bitcast.98, bf16[1024,512]{1,0:T(8,128)(2,1)} %all-gather.13.cloned.1.call-done), kind=kOutput, calls=%fused_computation.38 | convolution fusion | flops 671744000 | bytes 4325376 | tf_op jit(solution)/shard_map/dot_general | solution.py:212
  286.1 6.5 %reduce-scatter.5.cloned.1.call-done = bf16[320,512]{1,0:T(8,128)(2,1)} async-done(((bf16[640,512]{1,0:T(8,128)(2,1)}), bf16[320,512]{1,0:T(8,128)(2,1)}) %reduce-scatter.5.cloned.1.call-update) | async-done | bytes 327696 | tf_op jit(solution)/shard_map/reduce_scatter | solution.py:209
  292.6 11.0 %all_to_all.15 = bf16[4,80,512]{2,1,0:T(8,128)(2,1)S(1)} all-to-all(bf16[4,80,512]{2,1,0:T(8,128)(2,1)} %bitcast.107), channel_id=1, replica_groups=mesh['sp'=4,'fs'=4,'tp'=2] {'fs'}, dimensions={0} | all-to-all | bytes 655360 | tf_op jit(solution)/shard_map/all_to_all | solution.py:220
  (107 shorter events, 38.7 us)
Async XLA Ops:
  6.5 196.5 %copy-start = (bf16[512,1024]{1,0:T(8,128)(2,1)S(1)}, bf16[512,1024]{1,0:T(8,128)(2,1)}, u32[]{:S(2)}) copy-start(bf16[512,1024]{1,0:T(8,128)(2,1)} %param.29) | copy-start | bytes 3145732
  6.5 5.6 %copy-start.9 = (bf16[128,512]{1,0:T(8,128)(2,1)S(1)}, bf16[128,512]{1,0:T(8,128)(2,1)}, u32[]{:S(2)}) copy-start(bf16[128,512]{1,0:T(8,128)(2,1)} %param.20) | copy-start | bytes 393220
  6.5 23.1 %copy-start.10 = (bf16[128,512]{1,0:T(8,128)(2,1)S(1)}, bf16[128,512]{1,0:T(8,128)(2,1)}, u32[]{:S(2)}) copy-start(bf16[128,512]{1,0:T(8,128)(2,1)} %param.21) | copy-start | bytes 393220
  6.5 39.6 %copy-start.11 = (bf16[128,512]{1,0:T(8,128)(2,1)S(1)}, bf16[128,512]{1,0:T(8,128)(2,1)}, u32[]{:S(2)}) copy-start(bf16[128,512]{1,0:T(8,128)(2,1)} %param.22) | copy-start | bytes 393220
  6.5 96.9 %all-gather.7.cloned.1.call-start = ((), (), s32[]{:S(2)}) async-start(), calls=%async_computation.3 | async-start | bytes 3276800 | tf_op jit(solution)/shard_map/all_gather | solution.py:73
  9.3 53.5 %copy-start.12 = (bf16[128,512]{1,0:T(8,128)(2,1)S(1)}, bf16[128,512]{1,0:T(8,128)(2,1)}, u32[]{:S(2)}) copy-start(bf16[128,512]{1,0:T(8,128)(2,1)} %param.25) | copy-start | bytes 393220
  9.3 76.3 %copy-start.13 = (bf16[128,512]{1,0:T(8,128)(2,1)S(1)}, bf16[128,512]{1,0:T(8,128)(2,1)}, u32[]{:S(2)}) copy-start(bf16[128,512]{1,0:T(8,128)(2,1)} %param.26) | copy-start | bytes 393220
  11.4 109.0 %all-gather.9.cloned.1.call-start = ((), (), s32[]{:S(2)}) async-start(), calls=%async_computation.4 | async-start | bytes 1310720 | tf_op jit(solution)/shard_map/all_gather | solution.py:81
  12.1 168.6 %reduce-scatter.3.cloned.1.call-start = ((), (), s32[]{:S(2)}) async-start(), calls=%async_computation.5 | async-start | bytes 5734400 | tf_op jit(solution)/shard_map/reduce_scatter | solution.py:92
  109.0 4.8 %copy-start.5 = (bf16[640,4,1,128]{0,3,2,1:T(8,128)(2,1)}, bf16[640,4,1,128]{0,3,2,1:T(8,128)(2,1)S(1)}, u32[]{:S(2)}) copy-start(bf16[640,4,1,128]{0,3,2,1:T(8,128)(2,1)S(1)} %constant_dynamic-slice_fusion) | copy-start | bytes 1966084
  118.5 1.8 copy-start.6
  120.4 4.7 %copy-start.7 = (bf16[512,512]{1,0:T(8,128)(2,1)S(1)}, bf16[512,512]{1,0:T(8,128)(2,1)}, u32[]{:S(2)}) copy-start(bf16[512,512]{1,0:T(8,128)(2,1)} %all_gather.49) | copy-start | bytes 1572868
  126.5 1.1 copy-start.8
  126.5 55.3 %copy-start.17 = (f32[512]{0:T(512)S(1)}, f32[512]{0:T(512)}, u32[]{:S(2)}) copy-start(f32[512]{0:T(512)} %param.28) | copy-start | bytes 6148
  126.5 127.1 %all-gather.11.cloned.1.call-start = ((), (), s32[]{:S(2)}) async-start(), calls=%async_computation.6 | async-start | bytes 1638400 | tf_op jit(solution)/shard_map/all_gather | solution.py:193
  211.6 1.7 copy-start.1
  215.1 1.5 copy-start.2
  216.7 2.1 copy-start.18
  218.8 2.8 copy-start.15
  218.8 2.8 copy-start.4
  218.8 5.3 %copy-start.14 = (bf16[512,128]{1,0:T(8,128)(2,1)S(1)}, bf16[512,128]{1,0:T(8,128)(2,1)}, u32[]{:S(2)}) copy-start(bf16[512,128]{1,0:T(8,128)(2,1)} %param.32) | copy-start | bytes 393220
  220.9 61.9 %all-gather.13.cloned.1.call-start = ((), (), s32[]{:S(2)}) async-start(), calls=%async_computation.7 | async-start | bytes 1310720 | tf_op jit(solution)/shard_map/all_gather | solution.py:207
  221.5 71.1 %reduce-scatter.5.cloned.1.call-start = ((), (), s32[]{:S(2)}) async-start(), calls=%async_computation.8 | async-start | bytes 983040 | tf_op jit(solution)/shard_map/reduce_scatter | solution.py:209
  221.6 17.9 %collective-permute-start = (bf16[2,512]{1,0:T(2,128)(2,1)S(1)}, bf16[2,512]{1,0:T(2,128)(2,1)S(1)}, u32[]{:S(2)}, u32[]{:S(2)}) collective-permute-start(bf16[2,512]{1,0:T(2,128)(2,1)S(1)} %slice.44), channel_id=1, source_target_pairs={{0,8},{8,16},{16,24},{1,9},{9,17},{17,25},{2,10},{10,18},{18,26},{... | collective-permute-start | bytes 6152 | tf_op jit(solution)/shard_map/ppermute | solution.py:18
  (2 other events, 2.2 us)
Sparse Core Ops, SparseCore 0:
  11.5 42.1 all-gather.6
  55.2 39.4 all-gather.8
  126.6 54.0 reduce-scatter.2
  221.0 30.3 all-gather.10
  252.8 29.8 all-gather.12
  286.2 6.3 reduce-scatter.4
where the time goes:
time: 313 us; the launch traced here: 312 us
  blocking collectives  165 us (53%)
  waiting for transfers between devices  70.9 us (23%)
  local copies, waits for them, and re-layouts  23.9 us (8%)
  matrix products  23.6 us (8%)
  between operations  13.8 us (4%)
  other arithmetic  12 us (4%)
    reduce_scatter x1, waiting for transfers between devices, shards(): lax.psum_scatter(project_in().astype(jnp.bfloat16), 'fs', scatter_dimensi...  36.4 us
    all_gather x1, waiting for transfers between devices, shards(): lax.all_gather(attn_out_weight, 'sp', axis=1, tiled=True)  26.6 us
    all_gather x1, blocking collectives, shards(): lax.all_gather(query_rope_weight, 'sp', axis=0, tiled=True)  22.8 us
    all_gather x1, blocking collectives, shards(): lax.all_gather(latent_weight, 'sp', axis=0, tiled=True)  17.8 us
    all_gather x1, blocking collectives, shards(): latent_piece = lax.all_gather(latent, 'sp', axis=0, tiled=True)  17.8 us
    all_gather x1, blocking collectives, shards(): lax.all_gather(conv_b_weight, 'sp', axis=0, tiled=True)  17.5 us
    all_gather x1, blocking collectives, shards(): lax.all_gather(conv_v_weight, 'sp', axis=0, tiled=True)  16.7 us
    all_gather x1, blocking collectives, shards(): lax.all_gather(conv_c_weight, 'sp', axis=0, tiled=True)  16.5 us
  transfers between devices with their start and end apart: 7, of which 3 were waited for; matrix products, arithmetic and copies ran while one was open for 8% of the time, Pallas kernels for 0%

commit v1 on v0

--- a/solution.py
+++ b/solution.py
@@ -204,7 +204,7 @@
     )
     conv_cols_sp, attn_cols_sp = (
         lax.all_gather(conv_out_weight, "sp", axis=1, tiled=True),
-        lax.all_gather(attn_out_weight, "sp", axis=1, tiled=True),
+        jnp.concatenate(jax.lax.all_gather(attn_out_weight, "sp"), 1),
     )
     col_sums = lax.psum_scatter(
         (

time: 313 us -> 293 us (0.936)
  waiting for transfers between devices: 70.9 us -> 43.5 us
  blocking collectives: 165 us -> 171 us
    all_gather x1, waiting for transfers between devices: 26.6 us -> 0.01 us  [shards(): jax.lax.all_gather(attn_out_weight, 'sp')]
    all_gather x1, blocking collectives: 17.8 us -> 24.1 us  [shards(): latent_piece = lax.all_gather(latent, 'sp', axis=0, tiled=True)]
  transfers between devices with their start and end apart: 7 -> 7, of which waited for: 3 -> 2; matrix products, arithmetic and copies ran while one was open for 8% -> 15% of each run, Pallas kernels for 0% -> 0%
where the time goes in v1:
time: 293 us; the launch traced here: 292 us
  blocking collectives  171 us (58%)
  waiting for transfers between devices  43.5 us (15%)
  local copies, waits for them, and re-layouts  24.7 us (8%)
  matrix products  23.3 us (8%)
  between operations  13.8 us (5%)
  other arithmetic  12 us (4%)
  starting transfers between devices  3.08 us (1%)
    reduce_scatter x1, waiting for transfers between devices, shards(): lax.psum_scatter(project_in().astype(jnp.bfloat16), 'fs', scatter_dimensi...  36.4 us
    all_gather x1, blocking collectives, shards(): latent_piece = lax.all_gather(latent, 'sp', axis=0, tiled=True)  24.1 us
    all_gather x1, blocking collectives, shards(): lax.all_gather(query_rope_weight, 'sp', axis=0, tiled=True)  22.8 us
    all_gather x1, blocking collectives, shards(): lax.all_gather(latent_weight, 'sp', axis=0, tiled=True)  17.8 us
    all_gather x1, blocking collectives, shards(): lax.all_gather(conv_b_weight, 'sp', axis=0, tiled=True)  17.5 us
    all_gather x1, blocking collectives, shards(): lax.all_gather(conv_v_weight, 'sp', axis=0, tiled=True)  16.7 us
    all_gather x1, blocking collectives, shards(): lax.all_gather(conv_c_weight, 'sp', axis=0, tiled=True)  16.5 us
    all_gather x1, blocking collectives, shards(): lax.all_gather(conv_out_weight, 'sp', axis=1, tiled=True)  15.8 us
  transfers between devices with their start and end apart: 7, of which 2 were waited for; matrix products, arithmetic and copies ran while one was open for 15% of the time, Pallas kernels for 0%

profile of v1, /device:TPU:0, one launch (start us, length us, event | category | flops | bytes accessed | tf_op | source)
XLA Modules:
  0.0 291.5 jit_solution(10457387778085153424)
XLA Ops:
  6.6 2.7 all-gather
  12.2 17.5 %all_gather.47 = bf16[512,512]{1,0:T(8,128)(2,1)S(1)} all-gather(bf16[128,512]{1,0:T(8,128)(2,1)S(1)} %copy-done.9), channel_id=1, replica_groups=mesh['sp'=4,'fs'=4,'tp'=2] {'sp'}, dimensions={0}, use_global_device_ids=true | all-gather | bytes 655360 | tf_op jit(solution)/shard_map/all_gather | solution.py:78
  29.6 16.5 %all_gather.48 = bf16[512,512]{1,0:T(8,128)(2,1)} all-gather(bf16[128,512]{1,0:T(8,128)(2,1)S(1)} %copy-done.10), channel_id=1, replica_groups=mesh['sp'=4,'fs'=4,'tp'=2] {'sp'}, dimensions={0}, use_global_device_ids=true | all-gather | bytes 655360 | tf_op jit(solution)/shard_map/all_gather | solution.py:79
  46.1 16.7 %all_gather.49 = bf16[512,512]{1,0:T(8,128)(2,1)} all-gather(bf16[128,512]{1,0:T(8,128)(2,1)S(1)} %copy-done.11), channel_id=1, replica_groups=mesh['sp'=4,'fs'=4,'tp'=2] {'sp'}, dimensions={0}, use_global_device_ids=true | all-gather | bytes 655360 | tf_op jit(solution)/shard_map/all_gather | solution.py:80
  62.8 22.8 %all_gather.51 = bf16[512,512]{1,0:T(8,128)(2,1)S(1)} all-gather(bf16[128,512]{1,0:T(8,128)(2,1)S(1)} %copy-done.12), channel_id=1, replica_groups=mesh['sp'=4,'fs'=4,'tp'=2] {'sp'}, dimensions={0}, use_global_device_ids=true | all-gather | bytes 655360 | tf_op jit(solution)/shard_map/all_gather | solution.py:82
  85.6 17.8 %all_gather.52 = bf16[512,512]{1,0:T(8,128)(2,1)} all-gather(bf16[128,512]{1,0:T(8,128)(2,1)S(1)} %copy-done.13), channel_id=1, replica_groups=mesh['sp'=4,'fs'=4,'tp'=2] {'sp'}, dimensions={0}, use_global_device_ids=true | all-gather | bytes 655360 | tf_op jit(solution)/shard_map/all_gather | solution.py:83
  103.4 4.4 %copy.66 = bf16[640,2048]{0,1:T(8,128)(2,1)} copy(bf16[640,2048]{1,0:T(8,128)(2,1)} %all-gather.8.cloned.1.call-done) | data formatting | bytes 5242880 | tf_op jit(solution)/shard_map/all_gather | solution.py:73
  109.9 2.5 convolution_convert_fusion.5
  113.8 2.5 convolution_convert_fusion.4
  120.4 3.3 %fusion.15 = bf16[640,3584]{1,0:T(8,128)(2,1)} fusion(bf16[640,3584]{1,0:T(8,128)(2,1)} %constant_dynamic-update-slice_fusion, bf16[640,512]{0,1:T(8,128)(2,1)S(1)} %bitcast.110, bf16[512,1024]{1,0:T(8,128)(2,1)} %all-gather.10.cloned.1.call-done), kind=kOutput, calls=%fused_computation.35 | convolution fusion | flops 671744000 | bytes 3014656 | tf_op jit(solution)/shard_map/dot_general | solution.py:88
  128.4 14.1 %all-gather.2 = bf16[4,160,64]{1,2,0:T(8,128)(2,1)} all-gather(bf16[1,160,64]{1,2,0:T(8,128)(2,1)S(1)} %maximum_bitcast_fusion), channel_id=1, replica_groups=mesh['sp'=4,'fs'=4,'tp'=2] {'sp'}, dimensions={0}, use_global_device_ids=true | all-gather | bytes 102400 | tf_op jit(solution)/shard_map/all_gather | solution.py:161
  142.5 1.9 broadcast_in_dim.56
  144.3 36.4 %reduce-scatter.3.cloned.1.call-done = bf16[160,3584]{1,0:T(8,128)(2,1)} async-done(((bf16[640,3584]{1,0:T(8,128)(2,1)}), bf16[160,3584]{1,0:T(8,128)(2,1)}) %reduce-scatter.3.cloned.1.call-update) | async-done | bytes 1146896 | tf_op jit(solution)/shard_map/reduce_scatter | solution.py:92
  183.6 24.1 %all_gather.55 = bf16[640,512]{1,0:T(8,128)(2,1)S(1)} all-gather(bf16[160,512]{1,0:T(8,128)(2,1)S(1)} %get-tuple-element.251), channel_id=1, replica_groups=mesh['sp'=4,'fs'=4,'tp'=2] {'sp'}, dimensions={0}, use_global_device_ids=true | all-gather | bytes 819200 | tf_op jit(solution)/shard_map/all_gather | solution.py:160
  210.8 12.1 %conditional.1 = ((f32[160,8]{1,0:T(8,128)S(1)}, f32[160,8,512]{2,1,0:T(8,128)})) conditional(s32[]{:T(128)} %convert_element_type.79, (f32[160,8]{1,0:T(8,128)S(1)}, f32[160,8,512]{2,1,0:T(8,128)}) %tuple.31, (s32[160]{0:T(256)S(1)}, s32[160]{0:T(256)S(1)}, s32[]{:T(128)}, bf16[160,8,512]{2,0,1:T(8,128)(2,1)S(1)}, ...), branch_computations={%region_3.4_spmd, %region_4.7_spmd.clone} | conditional | flops 1792195712 | bytes 46272084 | solution.py:172
  215.9 1.9 select_reduce_fusion
  222.9 2.1 divide_convert_fusion
  227.3 2.8 collective-permute-start
  230.1 15.8 %all_gather.54 = bf16[512,512]{1,0:T(8,128)(2,1)S(1)} all-gather(bf16[512,128]{1,0:T(8,128)(2,1)S(1)} %copy-done.14), channel_id=1, replica_groups=mesh['sp'=4,'fs'=4,'tp'=2] {'sp'}, dimensions={1}, use_global_device_ids=true | all-gather | bytes 655360 | tf_op jit(solution)/shard_map/all_gather | solution.py:206
  245.9 2.4 copy.83
  249.4 12.0 %all_gather.53 = bf16[640,512]{1,0:T(8,128)(2,1)S(1)} all-gather(bf16[160,512]{1,0:T(8,128)(2,1)S(1)} %fusion.40), channel_id=1, replica_groups=mesh['sp'=4,'fs'=4,'tp'=2] {'fs'}, dimensions={0}, use_global_device_ids=true | all-gather | bytes 819200 | tf_op jit(solution)/shard_map/all_gather | solution.py:192
  263.4 3.0 %fusion.17 = bf16[640,512]{1,0:T(8,128)(2,1)} fusion(f32[640,512]{1,0:T(8,128)S(1)} %fusion.44, bf16[640,1024]{1,0:T(8,128)(2,1)S(1)} %bitcast.102, bf16[1024,512]{0,1:T(8,128)(2,1)} %bitcast.106), kind=kOutput, calls=%fused_computation.38 | convolution fusion | flops 671744000 | bytes 4325376 | tf_op jit(solution)/shard_map/dot_general | solution.py:212
  266.4 5.8 %reduce-scatter.5.cloned.1.call-done = bf16[320,512]{1,0:T(8,128)(2,1)} async-done(((bf16[640,512]{1,0:T(8,128)(2,1)}), bf16[320,512]{1,0:T(8,128)(2,1)}) %reduce-scatter.5.cloned.1.call-update) | async-done | bytes 327696 | tf_op jit(solution)/shard_map/reduce_scatter | solution.py:209
  272.2 11.0 %all_to_all.15 = bf16[4,80,512]{2,1,0:T(8,128)(2,1)S(1)} all-to-all(bf16[4,80,512]{2,1,0:T(8,128)(2,1)} %bitcast.113), channel_id=1, replica_groups=mesh['sp'=4,'fs'=4,'tp'=2] {'fs'}, dimensions={0} | all-to-all | bytes 655360 | tf_op jit(solution)/shard_map/all_to_all | solution.py:220
  (108 shorter events, 37.6 us)
Async XLA Ops:
  6.5 202.8 %copy-start = (bf16[512,1024]{1,0:T(8,128)(2,1)S(1)}, bf16[512,1024]{1,0:T(8,128)(2,1)}, u32[]{:S(2)}) copy-start(bf16[512,1024]{1,0:T(8,128)(2,1)} %param.29) | copy-start | bytes 3145732
  6.5 5.6 %copy-start.9 = (bf16[128,512]{1,0:T(8,128)(2,1)S(1)}, bf16[128,512]{1,0:T(8,128)(2,1)}, u32[]{:S(2)}) copy-start(bf16[128,512]{1,0:T(8,128)(2,1)} %param.20) | copy-start | bytes 393220
  6.5 23.1 %copy-start.10 = (bf16[128,512]{1,0:T(8,128)(2,1)S(1)}, bf16[128,512]{1,0:T(8,128)(2,1)}, u32[]{:S(2)}) copy-start(bf16[128,512]{1,0:T(8,128)(2,1)} %param.21) | copy-start | bytes 393220
  6.5 39.6 %copy-start.11 = (bf16[128,512]{1,0:T(8,128)(2,1)S(1)}, bf16[128,512]{1,0:T(8,128)(2,1)}, u32[]{:S(2)}) copy-start(bf16[128,512]{1,0:T(8,128)(2,1)} %param.22) | copy-start | bytes 393220
  6.5 96.9 %all-gather.8.cloned.1.call-start = ((), (), s32[]{:S(2)}) async-start(), calls=%async_computation.3 | async-start | bytes 3276800 | tf_op jit(solution)/shard_map/all_gather | solution.py:73
  9.3 53.5 %copy-start.12 = (bf16[128,512]{1,0:T(8,128)(2,1)S(1)}, bf16[128,512]{1,0:T(8,128)(2,1)}, u32[]{:S(2)}) copy-start(bf16[128,512]{1,0:T(8,128)(2,1)} %param.25) | copy-start | bytes 393220
  9.3 76.3 %copy-start.13 = (bf16[128,512]{1,0:T(8,128)(2,1)S(1)}, bf16[128,512]{1,0:T(8,128)(2,1)}, u32[]{:S(2)}) copy-start(bf16[128,512]{1,0:T(8,128)(2,1)} %param.26) | copy-start | bytes 393220
  11.4 109.0 %all-gather.10.cloned.1.call-start = ((), (), s32[]{:S(2)}) async-start(), calls=%async_computation.4 | async-start | bytes 1310720 | tf_op jit(solution)/shard_map/all_gather | solution.py:81
  12.1 168.6 %reduce-scatter.3.cloned.1.call-start = ((), (), s32[]{:S(2)}) async-start(), calls=%async_computation.5 | async-start | bytes 5734400 | tf_op jit(solution)/shard_map/reduce_scatter | solution.py:92
  109.0 4.8 %copy-start.5 = (bf16[640,4,1,128]{0,3,2,1:T(8,128)(2,1)}, bf16[640,4,1,128]{0,3,2,1:T(8,128)(2,1)S(1)}, u32[]{:S(2)}) copy-start(bf16[640,4,1,128]{0,3,2,1:T(8,128)(2,1)S(1)} %constant_dynamic-slice_fusion) | copy-start | bytes 1966084
  118.5 1.8 copy-start.6
  120.4 4.7 %copy-start.7 = (bf16[512,512]{1,0:T(8,128)(2,1)S(1)}, bf16[512,512]{1,0:T(8,128)(2,1)}, u32[]{:S(2)}) copy-start(bf16[512,512]{1,0:T(8,128)(2,1)} %all_gather.52) | copy-start | bytes 1572868
  126.5 1.1 copy-start.8
  126.5 55.3 %copy-start.17 = (f32[512]{0:T(512)S(1)}, f32[512]{0:T(512)}, u32[]{:S(2)}) copy-start(f32[512]{0:T(512)} %param.28) | copy-start | bytes 6148
  126.5 119.4 %all-gather.14.cloned.1.call-start = ((), (), s32[]{:S(2)}) async-start(), calls=%async_computation.8 | async-start | bytes 1310720 | tf_op jit(solution)/shard_map/all_gather | solution.py:207
  127.1 134.9 %all-gather.12.cloned.1.call-start = ((), (), s32[]{:S(2)}) async-start(), calls=%async_computation.6 | async-start | bytes 1638400 | tf_op jit(solution)/shard_map/all_gather | solution.py:193
  217.8 1.7 copy-start.1
  221.4 1.5 copy-start.2
  222.9 2.1 copy-start.18
  225.1 2.2 copy-start.15
  225.1 2.2 copy-start.4
  225.1 5.1 %copy-start.14 = (bf16[512,128]{1,0:T(8,128)(2,1)S(1)}, bf16[512,128]{1,0:T(8,128)(2,1)}, u32[]{:S(2)}) copy-start(bf16[512,128]{1,0:T(8,128)(2,1)} %param.32) | copy-start | bytes 393220
  227.2 45.0 %reduce-scatter.5.cloned.1.call-start = ((), (), s32[]{:S(2)}) async-start(), calls=%async_computation.7 | async-start | bytes 983040 | tf_op jit(solution)/shard_map/reduce_scatter | solution.py:209
  227.3 21.0 %collective-permute-start = (bf16[2,512]{1,0:T(2,128)(2,1)S(1)}, bf16[2,512]{1,0:T(2,128)(2,1)S(1)}, u32[]{:S(2)}, u32[]{:S(2)}) collective-permute-start(bf16[2,512]{1,0:T(2,128)(2,1)S(1)} %slice.44), channel_id=1, source_target_pairs={{0,8},{8,16},{16,24},{1,9},{9,17},{17,25},{2,10},{10,18},{18,26},{... | collective-permute-start | bytes 6152 | tf_op jit(solution)/shard_map/ppermute | solution.py:18
  (2 other events, 2.2 us)
Sparse Core Ops, SparseCore 0:
  11.5 42.1 all-gather.7
  55.2 39.4 all-gather.9
  126.6 54.0 reduce-scatter.2
  182.2 33.7 all-gather.13
  227.3 31.1 all-gather.11
  266.6 5.6 reduce-scatter.4
